TPU v7x, 512 devices: a 4x2x32 block of a 4x8x32 slice. The times are simulated.
512 devices in a mesh: grp: 2 (over y), ep: 64 (over z, core), tp: 4 (over x).
Axes of the slice: x: 4, y: 2, z: 32, core: 2. Of those that a mesh axis runs over, the one named last changes fastest.
The devices are a block of a 4x8x32 slice.
Arguments:
- tokens: bfloat16 [49152, 2048], P(('grp', 'ep'), 'tp'), parts along dimension 0
- group_choice: int32 [49152], P(('grp', 'ep')), parts along dimension 0, may hold values from 0 to 7, as said below
- expert_choice: int32 [49152, 2], P(('grp', 'ep')), parts along dimension 0, may hold values from 0 to 7, as said below
- group_weight: float32 [49152], P(('grp', 'ep')), parts along dimension 0, may hold values from 0.3 to 1
- expert_weight: float32 [49152, 2], P(('grp', 'ep')), parts along dimension 0, may hold values from 0.1 to 1
- norm_gain: float32 [2048], replicated, may hold values from 0.1 to 1.9
- w_gate: bfloat16 [64, 2048, 1024], P('ep', None, 'tp'), may hold values from -0.125 to 0.125
- w_up: bfloat16 [64, 2048, 1024], P('ep', None, 'tp'), may hold values from -0.125 to 0.125
- w_down: bfloat16 [64, 1024, 2048], P('ep', None, 'tp'), may hold values from -0.1875 to 0.1875
Outputs:
- moe_out: bfloat16 [49152, 2048], P(('grp', 'ep'), 'tp'), parts along dimension 0
There are 2 independent parts, one for each index of `grp`. A program takes and returns all parts, laid end to end along the dimension named above; an argument that names none is the same for every part. Nothing has to cross between parts.
Inputs may be any that keep to these rules, and one draw needn't show every extreme that they name: `group_choice`: group of each token, 0 to 7; within each aligned block of 384 tokens (the tokens of one index of ep) every group is chosen by the same number of tokens. `expert_choice`: a token's two entries differ; within each aligned block of 384 tokens no expert (group with entry) is named by more than 18 tokens, and in every block one expert of each group, the same one in all blocks, is named by exactly 18 tokens.
All inputs are finite; a program needn't handle non-finite values.
Results may differ from a plain program's by a relative error of at most 0.0071.
Values may be sent and summed in bfloat16 or wider, within the bound.
A program may use at most 64 MiB of HBM per device.

v0:
```python
import jax
import jax.numpy as jnp
from jax import lax
from jax.sharding import Mesh
from jax.sharding import PartitionSpec as P

GRP_EP = ("grp", "g", "e")
EP = ("g", "e")
GROUP_SIZE = 8


def rank_before(marks):
    return jnp.cumsum(marks, -2) - marks


def body(
    tokens,
    group_choice,
    expert_choice,
    group_weight,
    expert_weight,
    norm_gain,
    w_gate,
    w_up,
    w_down,
):
    rows, width = tokens.shape
    groups = lax.axis_size("g")
    members = lax.axis_size("e")
    per_group = rows // groups
    mean_load = 2 * per_group // members
    capacity = mean_load + min(mean_load // 2, per_group - mean_load)
    model_width = norm_gain.shape[0]
    mixing = group_weight[:, None] * expert_weight / jnp.sum(expert_weight, -1, keepdims=True)
    group_marks = (group_choice[:, None] == jnp.arange(groups, dtype=jnp.int32)).astype(jnp.int32)
    place = group_choice * per_group + jnp.sum(rank_before(group_marks) * group_marks, 1)
    spots = jnp.arange(rows, dtype=jnp.int32)
    sort = spots[:, None] == place[None, :]
    values = tokens.astype(jnp.float32)
    squares = lax.all_gather(jnp.sum(values * values, -1), "tp", axis=0)
    inv_rms = lax.rsqrt(jnp.sum(squares, 0) / model_width + 1e-06)
    gain = lax.dynamic_slice_in_dim(norm_gain, lax.axis_index("tp") * width, width, 0)
    normed = (values * inv_rms[:, None] * gain[None, :]).astype(jnp.bfloat16)
    by_group = jnp.dot(
        sort.astype(jnp.bfloat16), normed, preferred_element_type=jnp.float32
    ).astype(jnp.bfloat16)
    facts = jnp.concatenate([expert_choice.astype(jnp.float32), mixing], -1)
    facts = jnp.dot(sort.astype(jnp.float32), facts, precision=lax.Precision.HIGHEST)
    landed = lax.all_to_all(
        by_group.reshape(groups, per_group, width), "g", 0, 0, tiled=True
    ).reshape(rows, width)
    facts = lax.all_to_all(facts.reshape(groups, per_group, 4), "g", 0, 0, tiled=True).reshape(
        rows, 4
    )
    chosen = facts[:, :2].astype(jnp.int32).reshape(groups, per_group, 2)
    blocks = jnp.arange(groups, dtype=jnp.int32)[:, None, None]
    kinds = jnp.arange(members, dtype=jnp.int32)
    marks = jnp.sum((chosen[..., None] == kinds).astype(jnp.int32), 2)
    ranks = rank_before(marks)
    seats = jnp.sum(jnp.where(chosen[..., None] == kinds, ranks[:, :, None, :], 0), -1)
    targets = (chosen * groups + blocks) * capacity + seats
    targets = targets.reshape(rows, 2)
    seats_all = members * groups * capacity
    places = jnp.arange(seats_all, dtype=jnp.int32)
    picks = [targets[None, :, k] == places[:, None] for k in range(2)]
    dispatch = (picks[0] | picks[1]).astype(jnp.bfloat16)
    buffer = jnp.dot(dispatch, landed, preferred_element_type=jnp.float32).astype(jnp.bfloat16)
    received = lax.all_to_all(
        buffer.reshape(members, groups * capacity, width), "e", 0, 0, tiled=True
    ).reshape(seats_all, width)
    piece = lax.all_gather(received, "tp", axis=1, tiled=True)
    gate = jnp.dot(piece, w_gate[0], preferred_element_type=jnp.float32)
    up = jnp.dot(piece, w_up[0], preferred_element_type=jnp.float32)
    hidden = (jax.nn.silu(gate) * up).astype(jnp.bfloat16)
    hidden = lax.all_gather(hidden, "tp", axis=1, tiled=True)
    result = jnp.dot(hidden, w_down[0], preferred_element_type=jnp.float32).astype(jnp.bfloat16)
    back = lax.all_to_all(
        result.reshape(members, groups * capacity, width), "e", 0, 0, tiled=True
    ).reshape(seats_all, width)
    mixed = jnp.zeros((rows, width), jnp.float32)
    for k in range(2):
        picker = (targets[:, k : k + 1] == places[None, :]).astype(jnp.bfloat16)
        picked = jnp.dot(picker, back, preferred_element_type=jnp.float32)
        mixed = mixed + facts[:, 2 + k : 3 + k] * picked
    home = lax.all_to_all(
        mixed.astype(jnp.bfloat16).reshape(groups, per_group, width), "g", 0, 0, tiled=True
    ).reshape(rows, width)
    unsort = place[:, None] == spots[None, :]
    return jnp.dot(unsort.astype(jnp.bfloat16), home, preferred_element_type=jnp.float32).astype(
        jnp.bfloat16
    )


def solution(mesh):
    members = GROUP_SIZE
    split = Mesh(
        mesh.devices.reshape(
            mesh.shape["grp"], mesh.shape["ep"] // members, members, mesh.shape["tp"]
        ),
        ("grp", "g", "e", "tp"),
    )
    placed = (
        P(GRP_EP, "tp"),
        P(GRP_EP),
        P(GRP_EP, None),
        P(GRP_EP),
        P(GRP_EP, None),
        P(),
        P(EP, None, "tp"),
        P(EP, None, "tp"),
        P(EP, None, "tp"),
    )
    return jax.shard_map(
        body, mesh=split, in_specs=placed, out_specs=P(GRP_EP, "tp"), check_vma=False
    )
```

profile of v0, /device:TPU:96, one launch (start us, length us, event | category | flops | bytes accessed | tf_op | source)
XLA Modules:
  0.0 404.2 jit_solution(10690738187043938088)
XLA Ops:
  6.5 0.0 copy-start
  6.6 0.8 convert_element_type.48
  7.3 0.7 fusion.29
  8.0 0.8 reduce-window.6
  8.9 0.2 slice_reduce_fusion
  9.1 0.8 fusion.28
  9.9 0.7 multiply_add_fusion.1
  10.6 0.7 reduce_sum.57
  11.3 0.7 multiply_divide_fusion
  12.0 0.4 fusion.20
  12.4 0.1 reshape.73
  12.5 0.7 reshape.92
  13.2 42.5 %all-to-all-start = ((f32[8,1,192]{2,1,0:T(1,128)}), f32[8,1,192]{2,1,0:T(1,128)S(1)}, u32[]{:S(2)}, u32[]{:S(2)}) async-start(f32[8,1,192]{2,1,0:T(1,128)} %reshape.92), calls=%async_computation | async-start | bytes 16384 | tf_op jit(solution)/shard_map/all_to_all | solution.py:52
  55.7 1.2 fusion.17
  56.9 11.4 %all-gather.1 = f32[4,1,384]{2,1,0:T(1,128)S(1)} all-gather(f32[1,1,384]{2,1,0:T(1,128)S(1)} %reshape.84), channel_id=2, replica_groups=mesh['grp'=2,'g'=8,'e'=8,'tp'=4] {'tp'}, dimensions={0}, use_global_device_ids=true | all-gather | bytes 7680 | tf_op jit(solution)/shard_map/all_gather | solution.py:40
  68.3 0.8 dynamic_slice.3
  69.1 2.2 convolution_convert_fusion.3
  71.3 6.7 %all-to-all-done = f32[8,1,192]{2,1,0:T(1,128)S(1)} async-done(((f32[8,1,192]{2,1,0:T(1,128)}), f32[8,1,192]{2,1,0:T(1,128)S(1)}, u32[]{:S(2)}, u32[]{:S(2)}) %all-to-all-start) | async-done | bytes 6176 | tf_op jit(solution)/shard_map/all_to_all | solution.py:52
  78.0 15.0 %all-to-all-start.1 = ((bf16[8,48,512]{2,1,0:T(8,128)(2,1)}), bf16[8,48,512]{2,1,0:T(8,128)(2,1)S(1)}, u32[]{:S(2)}, u32[]{:S(2)}) async-start(bf16[8,48,512]{2,1,0:T(8,128)(2,1)} %bitcast.3), calls=%async_computation.1 | async-start | bytes 786432 | tf_op jit(solution)/shard_map/all_to_all | solution.py:49
  92.9 0.1 all-gather.5.cloned.1.call-start
  93.0 0.1 add.42
  93.1 0.6 broadcast.44
  93.7 0.7 reduce.11
  94.4 0.1 reshape.93
  94.5 0.1 reshape.74
  94.6 0.1 eq.140
  94.7 0.1 copy.29
  94.8 3.8 reduce-window_subtract_fusion
  98.6 0.1 copy.31
  98.8 0.1 reduce_sum.60
  98.9 34.6 %all-to-all-done.1 = bf16[8,48,512]{2,1,0:T(8,128)(2,1)S(1)} async-done(((bf16[8,48,512]{2,1,0:T(8,128)(2,1)}), bf16[8,48,512]{2,1,0:T(8,128)(2,1)S(1)}, u32[]{:S(2)}, u32[]{:S(2)}) %all-to-all-start.1) | async-done | bytes 393248 | tf_op jit(solution)/shard_map/all_to_all | solution.py:49
  133.6 0.8 convolution_convert_fusion.1
  134.4 40.5 %all_to_all.25 = bf16[8,144,512]{2,1,0:T(8,128)(2,1)} all-to-all(bf16[8,144,512]{2,1,0:T(8,128)(2,1)S(1)} %bitcast.50), channel_id=1, replica_groups=mesh['grp'=2,'g'=8,'e'=8,'tp'=4] {'e'}, dimensions={0} | all-to-all | bytes 2359296 | tf_op jit(solution)/shard_map/all_to_all | solution.py:68
  174.9 0.0 copy-start.2
  174.9 0.1 all-gather.5.cloned.1.call-update
  174.9 0.0 copy-start.3
  175.0 0.1 all-gather.7.cloned.1.call-start
  175.0 52.6 %all-gather.5.cloned.1.call-done = bf16[1152,2048]{1,0:T(8,128)(2,1)} async-done(((bf16[1152,512]{1,0:T(8,128)(2,1)}), bf16[1152,2048]{1,0:T(8,128)(2,1)}) %all-gather.5.cloned.1.call-update) | async-done | bytes 4718608 | tf_op jit(solution)/shard_map/all_gather | solution.py:71
  227.7 0.0 copy-done.2
  227.7 0.0 copy-start.1
  227.7 3.9 fusion.11
  231.6 0.0 copy-done.3
  231.6 0.0 copy-done.1
  231.6 2.4 fusion
  234.0 0.1 all-gather.7.cloned.1.call-update
  234.0 53.1 %all-gather.7.cloned.1.call-done = bf16[1152,1024]{1,0:T(8,128)(2,1)} async-done(((bf16[1152,256]{1,0:T(8,128)(2,1)}), bf16[1152,1024]{1,0:T(8,128)(2,1)}) %all-gather.7.cloned.1.call-update) | async-done | bytes 2359312 | tf_op jit(solution)/shard_map/all_gather | solution.py:75
  287.2 0.0 copy-done
  287.2 4.1 %convolution_convert_fusion = bf16[1152,512]{1,0:T(8,128)(2,1)} fusion(bf16[1152,1024]{1,0:T(8,128)(2,1)} %all-gather.7.cloned.1.call-done, bf16[1,1024,512]{2,1,0:T(8,128)(2,1)S(1)} %copy-done), kind=kOutput, calls=%fused_computation | convolution fusion | flops 1208549376 | bytes 4587520 | tf_op jit(solution)/shard_map/dot_general | solution.py:76
  291.2 5.3 %all-to-all-start.3 = ((bf16[8,144,512]{2,1,0:T(8,128)(2,1)}), bf16[8,144,512]{2,1,0:T(8,128)(2,1)S(1)}, u32[]{:S(2)}, u32[]{:S(2)}) async-start(bf16[8,144,512]{2,1,0:T(8,128)(2,1)} %bitcast.10), calls=%async_computation.3 | async-start | bytes 2359296 | tf_op jit(solution)/shard_map/all_to_all | solution.py:77
  296.5 25.9 %all-to-all-done.3 = bf16[8,144,512]{2,1,0:T(8,128)(2,1)S(1)} async-done(((bf16[8,144,512]{2,1,0:T(8,128)(2,1)}), bf16[8,144,512]{2,1,0:T(8,128)(2,1)S(1)}, u32[]{:S(2)}, u32[]{:S(2)}) %all-to-all-start.3) | async-done | bytes 1179680 | tf_op jit(solution)/shard_map/all_to_all | solution.py:77
  322.4 0.7 fusion.7
  323.2 0.7 fusion.8
  323.9 72.3 %all_to_all.26 = bf16[8,48,512]{2,1,0:T(8,128)(2,1)S(1)} all-to-all(bf16[8,48,512]{2,1,0:T(8,128)(2,1)S(1)} %bitcast.52), channel_id=1, replica_groups=mesh['grp'=2,'g'=8,'e'=8,'tp'=4] {'g'}, dimensions={0} | all-to-all | bytes 786432 | tf_op jit(solution)/shard_map/all_to_all | solution.py:85
  396.2 1.2 convolution_convert_fusion.2
  (15 shorter events, 0.2 us)
Async XLA Ops:
  6.5 280.6 %copy-start = (bf16[1,1024,512]{2,1,0:T(8,128)(2,1)S(1)}, bf16[1,1024,512]{2,1,0:T(8,128)(2,1)}, u32[]{:S(2)}) copy-start(bf16[1,1024,512]{2,1,0:T(8,128)(2,1)} %param.17) | copy-start | bytes 3145732
  13.2 64.8 %all-to-all-start = ((f32[8,1,192]{2,1,0:T(1,128)}), f32[8,1,192]{2,1,0:T(1,128)S(1)}, u32[]{:S(2)}, u32[]{:S(2)}) async-start(f32[8,1,192]{2,1,0:T(1,128)} %reshape.92), calls=%async_computation | async-start | bytes 16384 | tf_op jit(solution)/shard_map/all_to_all | solution.py:52
  78.0 55.6 %all-to-all-start.1 = ((bf16[8,48,512]{2,1,0:T(8,128)(2,1)}), bf16[8,48,512]{2,1,0:T(8,128)(2,1)S(1)}, u32[]{:S(2)}, u32[]{:S(2)}) async-start(bf16[8,48,512]{2,1,0:T(8,128)(2,1)} %bitcast.3), calls=%async_computation.1 | async-start | bytes 786432 | tf_op jit(solution)/shard_map/all_to_all | solution.py:49
  92.9 134.7 %all-gather.5.cloned.1.call-start = ((), (), s32[]{:S(2)}) async-start(), calls=%async_computation.5 | async-start | bytes 5898240 | tf_op jit(solution)/shard_map/all_gather | solution.py:71
  174.9 52.8 %copy-start.2 = (bf16[1,2048,256]{2,1,0:T(8,128)(2,1)S(1)}, bf16[1,2048,256]{2,1,0:T(8,128)(2,1)}, u32[]{:S(2)}) copy-start(bf16[1,2048,256]{2,1,0:T(8,128)(2,1)} %param.15) | copy-start | bytes 3145732
  174.9 56.6 %copy-start.3 = (bf16[1,2048,256]{2,1,0:T(8,128)(2,1)S(1)}, bf16[1,2048,256]{2,1,0:T(8,128)(2,1)}, u32[]{:S(2)}) copy-start(bf16[1,2048,256]{2,1,0:T(8,128)(2,1)} %param.16) | copy-start | bytes 3145732
  175.0 112.2 %all-gather.7.cloned.1.call-start = ((), (), s32[]{:S(2)}) async-start(), calls=%async_computation.6 | async-start | bytes 2949120 | tf_op jit(solution)/shard_map/all_gather | solution.py:75
  227.7 3.9 copy-start.1
  291.2 31.2 %all-to-all-start.3 = ((bf16[8,144,512]{2,1,0:T(8,128)(2,1)}), bf16[8,144,512]{2,1,0:T(8,128)(2,1)S(1)}, u32[]{:S(2)}, u32[]{:S(2)}) async-start(bf16[8,144,512]{2,1,0:T(8,128)(2,1)} %bitcast.10), calls=%async_computation.3 | async-start | bytes 2359296 | tf_op jit(solution)/shard_map/all_to_all | solution.py:77
Sparse Core Ops, SparseCore 0:
  175.1 52.5 all-gather.4
  234.1 52.9 all-gather.6
where the time goes:
time: 405 us; the launch traced here: 404 us
  waiting for transfers between devices  173 us (43%)
  blocking collectives  124 us (31%)
  starting transfers between devices  62.9 us (16%)
  matrix products  16.3 us (4%)
  between operations  13.6 us (3%)
  other arithmetic  11 us (3%)
    all_to_all x1, blocking collectives, body(): lax.all_to_all(mixed.astype(jnp.bfloat16).reshape(groups, per_group, widt...  72.3 us
    all_gather x1, waiting for transfers between devices, body(): hidden = lax.all_gather(hidden, 'tp', axis=1, tiled=True)  53.1 us
    all_gather x1, waiting for transfers between devices, body(): piece = lax.all_gather(received, 'tp', axis=1, tiled=True)  52.6 us
    all_to_all x1, starting transfers between devices, body(): lax.all_to_all(facts.reshape(groups, per_group, 4), 'g', 0, 0, tiled=True)  42.5 us
    all_to_all x1, blocking collectives, body(): lax.all_to_all(buffer.reshape(members, groups * capacity, width), 'e', 0,...  40.5 us
    all_to_all x1, waiting for transfers between devices, body(): lax.all_to_all(by_group.reshape(groups, per_group, width), 'g', 0, 0, til...  34.6 us
    all_to_all x1, waiting for transfers between devices, body(): lax.all_to_all(result.reshape(members, groups * capacity, width), 'e', 0,...  25.9 us
    all_to_all x1, starting transfers between devices, body(): lax.all_to_all(by_group.reshape(groups, per_group, width), 'g', 0, 0, til...  15 us
  transfers between devices with their start and end apart: 5, of which 5 were waited for; matrix products, arithmetic and copies ran while one was open for 2% of the time, Pallas kernels for 0%

commit v1 on v0

--- a/solution.py
+++ b/solution.py
@@ -72,7 +72,9 @@
     gate = jnp.dot(piece, w_gate[0], preferred_element_type=jnp.float32)
     up = jnp.dot(piece, w_up[0], preferred_element_type=jnp.float32)
     hidden = (jax.nn.silu(gate) * up).astype(jnp.bfloat16)
-    hidden = lax.all_gather(hidden, "tp", axis=1, tiled=True)
+    hidden = jnp.concatenate(
+        lax.all_to_all(jnp.stack([hidden] * lax.axis_size("tp")), "tp", 0, 0), axis=1
+    )
     result = jnp.dot(hidden, w_down[0], preferred_element_type=jnp.float32).astype(jnp.bfloat16)
     back = lax.all_to_all(
         result.reshape(members, groups * capacity, width), "e", 0, 0, tiled=True

time: 405 us -> 382 us (0.943)
  waiting for transfers between devices: 173 us -> 120 us
  blocking collectives: 124 us -> 156 us
    all_gather x1 -> x0, waiting for transfers between devices: 53.1 us -> none  [body(): hidden = lax.all_gather(hidden, 'tp', axis=1, tiled=True)]
    all_to_all x0 -> x1, blocking collectives: none -> 32.2 us  [body(): lax.all_to_all(jnp.stack([hidden] * lax.axis_size('tp')), 'tp', 0, 0)]
  transfers between devices with their start and end apart: 5 -> 4, of which waited for: 5 -> 4; matrix products, arithmetic and copies ran while one was open for 2% -> 3% of each run, Pallas kernels for 0% -> 0%
where the time goes in v1:
time: 382 us; the launch traced here: 381 us
  blocking collectives  156 us (41%)
  waiting for transfers between devices  120 us (31%)
  starting transfers between devices  62.9 us (16%)
  matrix products  13.9 us (4%)
  between operations  13.6 us (4%)
  other arithmetic  11 us (3%)
    all_to_all x1, blocking collectives, body(): lax.all_to_all(mixed.astype(jnp.bfloat16).reshape(groups, per_group, widt...  72.3 us
    all_gather x1, waiting for transfers between devices, body(): piece = lax.all_gather(received, 'tp', axis=1, tiled=True)  52.7 us
    all_to_all x1, starting transfers between devices, body(): lax.all_to_all(facts.reshape(groups, per_group, 4), 'g', 0, 0, tiled=True)  42.5 us
    all_to_all x1, blocking collectives, body(): lax.all_to_all(buffer.reshape(members, groups * capacity, width), 'e', 0,...  40.5 us
    all_to_all x1, waiting for transfers between devices, body(): lax.all_to_all(by_group.reshape(groups, per_group, width), 'g', 0, 0, til...  34.6 us
    all_to_all x1, blocking collectives, body(): lax.all_to_all(jnp.stack([hidden] * lax.axis_size('tp')), 'tp', 0, 0)  32.2 us
    all_to_all x1, waiting for transfers between devices, body(): lax.all_to_all(result.reshape(members, groups * capacity, width), 'e', 0,...  25.9 us
    all_to_all x1, starting transfers between devices, body(): lax.all_to_all(by_group.reshape(groups, per_group, width), 'g', 0, 0, til...  15 us
  transfers between devices with their start and end apart: 4, of which 4 were waited for; matrix products, arithmetic and copies ran while one was open for 3% of the time, Pallas kernels for 0%

profile of v1, /device:TPU:96, one launch (start us, length us, event | category | flops | bytes accessed | tf_op | source)
XLA Modules:
  0.0 381.3 jit_solution(2765265813732491599)
XLA Ops:
  6.5 0.0 copy-start
  6.6 0.8 convert_element_type.48
  7.3 0.7 fusion.29
  8.0 0.8 reduce-window.6
  8.9 0.2 slice_reduce_fusion
  9.1 0.8 fusion.28
  9.9 0.7 multiply_add_fusion.1
  10.6 0.7 reduce_sum.57
  11.3 0.7 multiply_divide_fusion
  12.0 0.4 fusion.20
  12.4 0.1 reshape.81
  12.5 0.7 reshape.102
  13.2 42.5 %all-to-all-start = ((f32[8,1,192]{2,1,0:T(1,128)}), f32[8,1,192]{2,1,0:T(1,128)S(1)}, u32[]{:S(2)}, u32[]{:S(2)}) async-start(f32[8,1,192]{2,1,0:T(1,128)} %reshape.102), calls=%async_computation | async-start | bytes 16384 | tf_op jit(solution)/shard_map/all_to_all | solution.py:52
  55.7 1.2 fusion.17
  56.9 11.4 %all-gather.1 = f32[4,1,384]{2,1,0:T(1,128)S(1)} all-gather(f32[1,1,384]{2,1,0:T(1,128)S(1)} %reshape.94), channel_id=2, replica_groups=mesh['grp'=2,'g'=8,'e'=8,'tp'=4] {'tp'}, dimensions={0}, use_global_device_ids=true | all-gather | bytes 7680 | tf_op jit(solution)/shard_map/all_gather | solution.py:40
  68.3 0.8 dynamic_slice.3
  69.1 2.2 convolution_convert_fusion.3
  71.3 6.7 %all-to-all-done = f32[8,1,192]{2,1,0:T(1,128)S(1)} async-done(((f32[8,1,192]{2,1,0:T(1,128)}), f32[8,1,192]{2,1,0:T(1,128)S(1)}, u32[]{:S(2)}, u32[]{:S(2)}) %all-to-all-start) | async-done | bytes 6176 | tf_op jit(solution)/shard_map/all_to_all | solution.py:52
  78.0 15.0 %all-to-all-start.1 = ((bf16[8,48,512]{2,1,0:T(8,128)(2,1)}), bf16[8,48,512]{2,1,0:T(8,128)(2,1)S(1)}, u32[]{:S(2)}, u32[]{:S(2)}) async-start(bf16[8,48,512]{2,1,0:T(8,128)(2,1)} %bitcast.3), calls=%async_computation.1 | async-start | bytes 786432 | tf_op jit(solution)/shard_map/all_to_all | solution.py:49
  92.9 0.1 all-gather.4.cloned.1.call-start
  93.0 0.1 add.42
  93.1 0.6 broadcast.46
  93.7 0.7 reduce.11
  94.4 0.1 reshape.103
  94.5 0.1 reshape.82
  94.6 0.1 eq.140
  94.7 0.1 copy.33
  94.8 3.8 reduce-window_subtract_fusion
  98.6 0.1 copy.35
  98.8 0.1 reduce_sum.60
  98.9 34.6 %all-to-all-done.1 = bf16[8,48,512]{2,1,0:T(8,128)(2,1)S(1)} async-done(((bf16[8,48,512]{2,1,0:T(8,128)(2,1)}), bf16[8,48,512]{2,1,0:T(8,128)(2,1)S(1)}, u32[]{:S(2)}, u32[]{:S(2)}) %all-to-all-start.1) | async-done | bytes 393248 | tf_op jit(solution)/shard_map/all_to_all | solution.py:49
  133.6 0.8 convolution_convert_fusion.1
  134.4 40.5 %all_to_all.30 = bf16[8,144,512]{2,1,0:T(8,128)(2,1)} all-to-all(bf16[8,144,512]{2,1,0:T(8,128)(2,1)S(1)} %bitcast.54), channel_id=1, replica_groups=mesh['grp'=2,'g'=8,'e'=8,'tp'=4] {'e'}, dimensions={0} | all-to-all | bytes 2359296 | tf_op jit(solution)/shard_map/all_to_all | solution.py:68
  174.9 0.0 copy-start.2
  174.9 0.1 all-gather.4.cloned.1.call-update
  174.9 0.0 copy-start.3
  175.0 52.7 %all-gather.4.cloned.1.call-done = bf16[1152,2048]{1,0:T(8,128)(2,1)} async-done(((bf16[1152,512]{1,0:T(8,128)(2,1)}), bf16[1152,2048]{1,0:T(8,128)(2,1)}) %all-gather.4.cloned.1.call-update) | async-done | bytes 4718608 | tf_op jit(solution)/shard_map/all_gather | solution.py:71
  227.7 0.0 copy-done.2
  227.7 0.0 copy-start.1
  227.7 3.9 %fusion.11 = f32[1152,256]{1,0:T(8,128)S(1)} fusion(bf16[1152,2048]{1,0:T(8,128)(2,1)} %all-gather.4.cloned.1.call-done, bf16[1,2048,256]{2,1,0:T(8,128)(2,1)S(1)} %copy-done.2), kind=kOutput, calls=%fused_computation.20 | convolution fusion | flops 1207959552 | bytes 6946816 | tf_op jit(solution)/shard_map/dot_general | solution.py:72
  231.6 0.0 copy-done.3
  231.6 0.0 copy-done.1
  231.6 1.6 fusion
  233.1 0.3 copy.37
  233.4 0.2 stack.2
  233.6 32.2 %all_to_all.31 = bf16[4,1152,256]{1,2,0:T(8,128)(2,1)S(1)} all-to-all(bf16[4,1152,256]{1,2,0:T(8,128)(2,1)S(1)} %stack.2), channel_id=1, replica_groups=mesh['grp'=2,'g'=8,'e'=8,'tp'=4] {'tp'}, dimensions={0} | all-to-all | bytes 4718592 | tf_op jit(solution)/shard_map/all_to_all | solution.py:76
  265.8 0.0 copy-done
  265.8 2.4 convolution_convert_fusion
  268.2 5.3 %all-to-all-start.4 = ((bf16[8,144,512]{2,1,0:T(8,128)(2,1)}), bf16[8,144,512]{2,1,0:T(8,128)(2,1)S(1)}, u32[]{:S(2)}, u32[]{:S(2)}) async-start(bf16[8,144,512]{2,1,0:T(8,128)(2,1)} %bitcast.12), calls=%async_computation.4 | async-start | bytes 2359296 | tf_op jit(solution)/shard_map/all_to_all | solution.py:79
  273.5 25.9 %all-to-all-done.4 = bf16[8,144,512]{2,1,0:T(8,128)(2,1)S(1)} async-done(((bf16[8,144,512]{2,1,0:T(8,128)(2,1)}), bf16[8,144,512]{2,1,0:T(8,128)(2,1)S(1)}, u32[]{:S(2)}, u32[]{:S(2)}) %all-to-all-start.4) | async-done | bytes 1179680 | tf_op jit(solution)/shard_map/all_to_all | solution.py:79
  299.5 0.7 fusion.7
  300.2 0.7 fusion.8
  300.9 72.3 %all_to_all.32 = bf16[8,48,512]{2,1,0:T(8,128)(2,1)S(1)} all-to-all(bf16[8,48,512]{2,1,0:T(8,128)(2,1)S(1)} %bitcast.56), channel_id=1, replica_groups=mesh['grp'=2,'g'=8,'e'=8,'tp'=4] {'g'}, dimensions={0} | all-to-all | bytes 786432 | tf_op jit(solution)/shard_map/all_to_all | solution.py:87
  373.2 1.2 convolution_convert_fusion.2
  (15 shorter events, 0.2 us)
Async XLA Ops:
  6.5 259.3 %copy-start = (bf16[1,1024,512]{2,1,0:T(8,128)(2,1)S(1)}, bf16[1,1024,512]{2,1,0:T(8,128)(2,1)}, u32[]{:S(2)}) copy-start(bf16[1,1024,512]{2,1,0:T(8,128)(2,1)} %param.17) | copy-start | bytes 3145732
  13.2 64.8 %all-to-all-start = ((f32[8,1,192]{2,1,0:T(1,128)}), f32[8,1,192]{2,1,0:T(1,128)S(1)}, u32[]{:S(2)}, u32[]{:S(2)}) async-start(f32[8,1,192]{2,1,0:T(1,128)} %reshape.102), calls=%async_computation | async-start | bytes 16384 | tf_op jit(solution)/shard_map/all_to_all | solution.py:52
  78.0 55.6 %all-to-all-start.1 = ((bf16[8,48,512]{2,1,0:T(8,128)(2,1)}), bf16[8,48,512]{2,1,0:T(8,128)(2,1)S(1)}, u32[]{:S(2)}, u32[]{:S(2)}) async-start(bf16[8,48,512]{2,1,0:T(8,128)(2,1)} %bitcast.3), calls=%async_computation.1 | async-start | bytes 786432 | tf_op jit(solution)/shard_map/all_to_all | solution.py:49
  92.9 134.7 %all-gather.4.cloned.1.call-start = ((), (), s32[]{:S(2)}) async-start(), calls=%async_computation.6 | async-start | bytes 5898240 | tf_op jit(solution)/shard_map/all_gather | solution.py:71
  174.9 52.8 %copy-start.2 = (bf16[1,2048,256]{2,1,0:T(8,128)(2,1)S(1)}, bf16[1,2048,256]{2,1,0:T(8,128)(2,1)}, u32[]{:S(2)}) copy-start(bf16[1,2048,256]{2,1,0:T(8,128)(2,1)} %param.15) | copy-start | bytes 3145732
  174.9 56.6 %copy-start.3 = (bf16[1,2048,256]{2,1,0:T(8,128)(2,1)S(1)}, bf16[1,2048,256]{2,1,0:T(8,128)(2,1)}, u32[]{:S(2)}) copy-start(bf16[1,2048,256]{2,1,0:T(8,128)(2,1)} %param.16) | copy-start | bytes 3145732
  227.7 3.9 %copy-start.1 = (bf16[1152,2048]{1,0:T(8,128)(2,1)S(1)}, bf16[1152,2048]{1,0:T(8,128)(2,1)}, u32[]{:S(2)}) copy-start(bf16[1152,2048]{1,0:T(8,128)(2,1)} %all-gather.4.cloned.1.call-done) | copy-start | bytes 14155780
  268.2 31.2 %all-to-all-start.4 = ((bf16[8,144,512]{2,1,0:T(8,128)(2,1)}), bf16[8,144,512]{2,1,0:T(8,128)(2,1)S(1)}, u32[]{:S(2)}, u32[]{:S(2)}) async-start(bf16[8,144,512]{2,1,0:T(8,128)(2,1)} %bitcast.12), calls=%async_computation.4 | async-start | bytes 2359296 | tf_op jit(solution)/shard_map/all_to_all | solution.py:79
Sparse Core Ops, SparseCore 0:
  175.1 52.5 all-gather.3
